TPU v7x, 32 devices: a whole 2x2x4 slice. The times are simulated.
32 devices in a mesh: grp: 2 (over y), sp: 4 (over z), tp: 4 (over x, core).
Axes of the slice: x: 2, y: 2, z: 4, core: 2. Of those that a mesh axis runs over, the one named last changes fastest.
Arguments:
- hidden_in: bfloat16 [5120, 4096], P(('grp', 'sp'), 'tp'), parts along dimension 0, may hold values from -64 to 64
- norm_gain: float32 [2, 4096], replicated, may hold values from 0.1 to 1.9
- w_pool_in: bfloat16 [2, 4096, 1024], P(None, 'sp', 'tp'), may hold values from -0.09375 to 0.09375
- w_pool_gate: bfloat16 [2, 4096, 1024], P(None, 'sp', 'tp'), may hold values from -0.09375 to 0.09375
- group_mix: bfloat16 [2, 16, 64, 64], replicated, may hold values from -0.75 to 0.75
- w_out: bfloat16 [2, 1024, 4096], P(None, 'sp', 'tp'), may hold values from -0.1875 to 0.1875
Outputs:
- hidden_out: bfloat16 [5120, 4096], P(('grp', 'sp'), 'tp'), parts along dimension 0
There are 2 independent parts, one for each index of `grp`. A program takes and returns all parts, laid end to end along the dimension named above; an argument that names none is the same for every part. Nothing has to cross between parts.
All inputs are finite; a program needn't handle non-finite values.
Results may differ from a plain program's by a relative error of at most 0.012.
Values may be sent and summed in bfloat16 or wider, within the bound.
A program may use at most 64 MiB of HBM per device.

v0:
```python
import jax
import jax.numpy as jnp
from jax import lax
from jax.sharding import PartitionSpec as P

GROUP = 64
norm_eps = 1e-06


def with_halo(array, sides, width):
    for axis, dim in sides:
        size, length = (lax.axis_size(axis), array.shape[dim])
        up = [(i, (i + 1) % size) for i in range(size - 1)]
        down = [(j, i) for i, j in up]
        last = lax.slice_in_dim(array, length - width, length, axis=dim)
        leading = lax.slice_in_dim(array, 0, width, axis=dim)
        before = lax.ppermute(last, axis, up)
        after = lax.ppermute(leading, axis, down)
        array = jnp.concatenate([before, array, after], axis=dim)
    return array


def local(hidden_in, norm_gain, w_pool_in, w_pool_gate, group_mix, w_out):
    tok_rows = hidden_in.shape[0]
    col_count = hidden_in.shape[1]
    chan_count = w_pool_in.shape[2]
    group_local = chan_count // GROUP
    layer_count = w_pool_in.shape[0]
    col_rank = lax.axis_index("tp")
    row_rank = lax.axis_index("sp")
    total_rows = tok_rows * lax.axis_size("sp")
    full_width = col_count * lax.axis_size("tp")
    position = row_rank * tok_rows + jnp.arange(tok_rows, dtype=jnp.int32)
    channel_code = (col_rank * group_local + jnp.arange(chan_count, dtype=jnp.int32) // GROUP) % 4
    every_in, every_gate, every_out = (
        lax.all_gather(w_pool_in, "sp", axis=1, tiled=True),
        lax.all_gather(w_pool_gate, "sp", axis=1, tiled=True),
        lax.all_gather(w_out, "sp", axis=1, tiled=True),
    )
    resid = hidden_in
    for layer in range(layer_count):
        weight_in = every_in[layer]
        weight_gate = every_gate[layer]
        weight_out = every_out[layer]
        resid_f = resid.astype(jnp.float32)
        squares = lax.psum(jnp.sum(resid_f * resid_f, axis=1), "tp")
        scaling = lax.rsqrt(squares / full_width + norm_eps)
        own_gain = lax.dynamic_slice_in_dim(norm_gain[layer], col_rank * col_count, col_count)
        normed = (resid_f * scaling[:, None] * own_gain[None, :]).astype(jnp.bfloat16)
        piece = lax.all_gather(normed, "tp", axis=1, tiled=True)
        pool_sum = jnp.dot(piece, weight_in, preferred_element_type=jnp.float32)
        gate_sum = jnp.dot(piece, weight_gate, preferred_element_type=jnp.float32)
        pool_in = pool_sum.astype(jnp.bfloat16)
        gate = gate_sum.astype(jnp.bfloat16)
        padded = with_halo(pool_in, (("sp", 0),), 8).astype(jnp.float32)
        running = jnp.zeros((tok_rows, chan_count), jnp.float32)
        averaged = jnp.zeros((tok_rows, chan_count), jnp.float32)
        previous = 0
        for code_value, half in enumerate((1, 2, 4, 8)):
            for offset in list(range(-half, -previous)) + list(range(previous, half)):
                running = running + padded[8 + offset : 8 + offset + tok_rows]
            previous = half
            counted = (
                jnp.minimum(position + half, total_rows) - jnp.maximum(position - half, 0)
            ).astype(jnp.float32)
            averaged = jnp.where(
                channel_code[None, :] == code_value, running / counted[:, None], averaged
            )
        pooled = (averaged - padded[8 : 8 + tok_rows]).astype(jnp.bfloat16)
        own_mix = lax.dynamic_slice_in_dim(group_mix[layer], col_rank * group_local, group_local, 0)
        mixed = jnp.einsum(
            "tgc,gcd->tgd",
            pooled.reshape(tok_rows, group_local, GROUP),
            own_mix,
            preferred_element_type=jnp.float32,
        ).reshape(tok_rows, chan_count)
        branch = (mixed * jax.nn.silu(gate.astype(jnp.float32))).astype(jnp.bfloat16)
        projected = jnp.dot(
            lax.all_gather(branch, "tp", axis=1, tiled=True),
            weight_out,
            preferred_element_type=jnp.float32,
        )
        resid = (resid_f + projected).astype(jnp.bfloat16)
    return resid


def solution(mesh):
    in_specs = (
        P(("grp", "sp"), "tp"),
        P(),
        P(None, "sp", "tp"),
        P(None, "sp", "tp"),
        P(),
        P(None, "sp", "tp"),
    )
    out_specs = P(("grp", "sp"), "tp")
    return jax.shard_map(local, mesh=mesh, in_specs=in_specs, out_specs=out_specs, check_vma=False)
```

profile of v0, /device:TPU:0, one launch (start us, length us, event | category | flops | bytes accessed | tf_op | source)
XLA Modules:
  0.0 417.1 jit_solution(7042506414387707074)
XLA Ops:
  6.5 0.7 all-gather.10.cloned.1.call-update
  7.3 1.6 fusion
  9.0 8.4 %psum.14 = f32[640]{0:T(1024)S(1)} all-reduce(f32[640]{0:T(1024)S(1)} %fusion), channel_id=1, replica_groups=mesh['grp'=2,'sp'=4,'tp'=4] {'tp'}, use_global_device_ids=true, to_apply=%region_1.2 | all-reduce | flops 640 | bytes 5120 | tf_op jit(solution)/shard_map/psum | solution.py:46
  17.3 0.9 fusion.41
  18.2 1.4 fusion.2
  19.7 0.7 all-gather.12.cloned.1.call-update
  20.5 0.5 all-gather.16.cloned.1.call-update
  21.2 71.2 %all-gather.10.cloned.1.call-done = bf16[2,4096,256]{2,1,0:T(8,128)(2,1)} async-done(((bf16[2,1024,256]{2,1,0:T(8,128)(2,1)}), bf16[2,4096,256]{2,1,0:T(8,128)(2,1)}) %all-gather.10.cloned.1.call-update) | async-done | bytes 4194320 | tf_op jit(solution)/shard_map/all_gather | solution.py:36
  92.4 40.5 %all-gather.8.cloned.1.call-done = bf16[640,4096]{1,0:T(8,128)(2,1)} async-done(((bf16[640,1024]{1,0:T(8,128)(2,1)}), bf16[640,4096]{1,0:T(8,128)(2,1)}) %all-gather.8.cloned.1.call-update) | async-done | bytes 5242896 | tf_op jit(solution)/shard_map/all_gather | solution.py:50
  132.9 4.7 %fusion.14 = bf16[640,256]{1,0:T(8,128)(2,1)S(1)} fusion(bf16[640,4096]{1,0:T(8,128)(2,1)} %all-gather.8.cloned.1.call-done, bf16[2,4096,256]{2,1,0:T(8,128)(2,1)} %all-gather.10.cloned.1.call-done), kind=kOutput, calls=%fused_computation.26 | convolution fusion | flops 1342341120 | bytes 7667712 | tf_op jit(solution)/shard_map/dot_general | solution.py:51
  137.6 3.4 collective-permute-start
  141.0 1.3 collective-permute-start.1
  142.3 4.2 %collective-permute-done.1 = bf16[8,256]{1,0:T(8,128)(2,1)S(1)} collective-permute-done((bf16[8,256]{1,0:T(8,128)(2,1)S(1)}, bf16[8,256]{1,0:T(8,128)(2,1)S(1)}, u32[]{:S(2)}, u32[]{:S(2)}) %collective-permute-start.1) | collective-permute-done | bytes 4128 | tf_op jit(solution)/shard_map/ppermute | solution.py:18
  146.5 1.5 fusion.26
  148.2 0.3 fusion.30
  148.7 66.5 %all-gather.12.cloned.1.call-done = bf16[2,4096,256]{2,1,0:T(8,128)(2,1)} async-done(((bf16[2,1024,256]{2,1,0:T(8,128)(2,1)}), bf16[2,4096,256]{2,1,0:T(8,128)(2,1)}) %all-gather.12.cloned.1.call-update) | async-done | bytes 4194320 | tf_op jit(solution)/shard_map/all_gather | solution.py:37
  215.3 5.4 %multiply_convert_fusion.1 = bf16[640,256]{1,0:T(8,128)(2,1)} fusion(f32[640,256]{1,0:T(8,128)S(1)} %copy.15, bf16[640,4096]{1,0:T(8,128)(2,1)} %all-gather.8.cloned.1.call-done, bf16[2,4096,256]{2,1,0:T(8,128)(2,1)} %all-gather.12.cloned.1.call-done), kind=kOutput, calls=%fused_computation.69 | convolution fusion | flops 1343488000 | bytes 8323072 | tf_op jit(solution)/shard_map/dot_general | solution.py:52
  220.8 75.1 %all-gather.16.cloned.1.call-done = bf16[2,1024,1024]{2,1,0:T(8,128)(2,1)} async-done(((bf16[2,256,1024]{2,1,0:T(8,128)(2,1)}), bf16[2,1024,1024]{2,1,0:T(8,128)(2,1)}) %all-gather.16.cloned.1.call-update) | async-done | bytes 4194320 | tf_op jit(solution)/shard_map/all_gather | solution.py:38
  295.9 18.2 %all-gather.14.cloned.1.call-done = bf16[640,1024]{1,0:T(8,128)(2,1)} async-done(((bf16[640,256]{1,0:T(8,128)(2,1)}), bf16[640,1024]{1,0:T(8,128)(2,1)}) %all-gather.14.cloned.1.call-update) | async-done | bytes 1310736 | tf_op jit(solution)/shard_map/all_gather | solution.py:79
  314.1 3.7 fusion.4
  317.8 5.9 %psum.15 = f32[640]{0:T(1024)S(1)} all-reduce(f32[640]{0:T(1024)S(1)} %get-tuple-element.13), channel_id=1, replica_groups=mesh['grp'=2,'sp'=4,'tp'=4] {'tp'}, use_global_device_ids=true, to_apply=%region_3.4 | all-reduce | flops 640 | bytes 5120 | tf_op jit(solution)/shard_map/psum | solution.py:46
  323.7 1.4 fusion.6
  325.2 41.6 %all-gather.18.cloned.1.call-done = bf16[640,4096]{1,0:T(8,128)(2,1)} async-done(((bf16[640,1024]{1,0:T(8,128)(2,1)}), bf16[640,4096]{1,0:T(8,128)(2,1)}) %all-gather.18.cloned.1.call-update) | async-done | bytes 5242896 | tf_op jit(solution)/shard_map/all_gather | solution.py:50
  366.8 4.7 %fusion.17 = bf16[640,256]{1,0:T(8,128)(2,1)S(1)} fusion(bf16[640,4096]{1,0:T(8,128)(2,1)} %all-gather.18.cloned.1.call-done, bf16[2,4096,256]{2,1,0:T(8,128)(2,1)} %all-gather.10.cloned.1.call-done), kind=kOutput, calls=%fused_computation.29 | convolution fusion | flops 1342341120 | bytes 7667712 | tf_op jit(solution)/shard_map/dot_general | solution.py:51
  371.5 3.4 collective-permute-start.2
  374.9 1.5 collective-permute-start.3
  376.4 4.0 collective-permute-done.3
  380.5 1.5 fusion.27
  382.1 0.3 fusion.28
  382.7 5.4 %multiply_convert_fusion = bf16[640,256]{1,0:T(8,128)(2,1)} fusion(f32[640,256]{1,0:T(8,128)S(1)} %copy.18, bf16[640,4096]{1,0:T(8,128)(2,1)} %all-gather.18.cloned.1.call-done, bf16[2,4096,256]{2,1,0:T(8,128)(2,1)} %all-gather.12.cloned.1.call-done), kind=kOutput, calls=%fused_computation.68 | convolution fusion | flops 1343488000 | bytes 8323072 | tf_op jit(solution)/shard_map/dot_general | solution.py:52
  388.1 17.6 %all-gather.20.cloned.1.call-done = bf16[640,1024]{1,0:T(8,128)(2,1)} async-done(((bf16[640,256]{1,0:T(8,128)(2,1)}), bf16[640,1024]{1,0:T(8,128)(2,1)}) %all-gather.20.cloned.1.call-update) | async-done | bytes 1310736 | tf_op jit(solution)/shard_map/all_gather | solution.py:79
  405.7 4.6 %fusion.7 = bf16[640,1024]{1,0:T(8,128)(2,1)} fusion(bf16[640,1024]{1,0:T(8,128)(2,1)S(1)} %get-tuple-element.14, bf16[640,1024]{1,0:T(8,128)(2,1)} %all-gather.20.cloned.1.call-done, bf16[2,1024,1024]{2,1,0:T(8,128)(2,1)} %all-gather.16.cloned.1.call-done), kind=kOutput, calls=%fused_computation.13 | convolution fusion | flops 1344143360 | bytes 6029312 | tf_op jit(solution)/shard_map/dot_general | solution.py:78
  (34 shorter events, 1.4 us)
Async XLA Ops:
  6.5 11.7 %copy-start = (bf16[640,1024]{1,0:T(8,128)(2,1)S(1)}, bf16[640,1024]{1,0:T(8,128)(2,1)}, u32[]{:S(2)}) copy-start(bf16[640,1024]{1,0:T(8,128)(2,1)} %param.6) | copy-start | bytes 3932164
  6.5 85.9 %all-gather.10.cloned.1.call-start = ((), (), s32[]{:S(2)}) async-start(), calls=%async_computation.1 | async-start | bytes 5242880 | tf_op jit(solution)/shard_map/all_gather | solution.py:36
  7.3 125.6 %all-gather.8.cloned.1.call-start = ((), (), s32[]{:S(2)}) async-start(), calls=%async_computation | async-start | bytes 6553600 | tf_op jit(solution)/shard_map/all_gather | solution.py:50
  18.2 2.9 copy-start.1
  19.7 195.6 %all-gather.12.cloned.1.call-start = ((), (), s32[]{:S(2)}) async-start(), calls=%async_computation.2 | async-start | bytes 5242880 | tf_op jit(solution)/shard_map/all_gather | solution.py:37
  20.4 275.5 %all-gather.16.cloned.1.call-start = ((), (), s32[]{:S(2)}) async-start(), calls=%async_computation.4 | async-start | bytes 5242880 | tf_op jit(solution)/shard_map/all_gather | solution.py:38
  21.0 293.1 %all-gather.14.cloned.1.call-start = ((), (), s32[]{:S(2)}) async-start(), calls=%async_computation.3 | async-start | bytes 1638400 | tf_op jit(solution)/shard_map/all_gather | solution.py:79
  137.6 4.7 %collective-permute-start = (bf16[8,256]{1,0:T(8,128)(2,1)S(1)}, bf16[8,256]{1,0:T(8,128)(2,1)S(1)}, u32[]{:S(2)}, u32[]{:S(2)}) collective-permute-start(bf16[8,256]{1,0:T(8,128)(2,1)S(1)} %get-tuple-element.9), channel_id=1, source_target_pairs={{0,4},{4,8},{8,12},{1,5},{5,9},{9,13},{2,6},{6,10},{10,14},{3,7},{... | collective-permute-start | bytes 12296 | tf_op jit(solution)/shard_map/ppermute | solution.py:17
  141.0 5.5 %collective-permute-start.1 = (bf16[8,256]{1,0:T(8,128)(2,1)S(1)}, bf16[8,256]{1,0:T(8,128)(2,1)S(1)}, u32[]{:S(2)}, u32[]{:S(2)}) collective-permute-start(bf16[8,256]{1,0:T(8,128)(2,1)S(1)} %get-tuple-element.10), channel_id=1, source_target_pairs={{4,0},{8,4},{12,8},{5,1},{9,5},{13,9},{6,2},{10,6},{14,10},{7,3},{... | collective-permute-start | bytes 12296 | tf_op jit(solution)/shard_map/ppermute | solution.py:18
  220.7 146.1 %all-gather.18.cloned.1.call-start = ((), (), s32[]{:S(2)}) async-start(), calls=%async_computation.5 | async-start | bytes 6553600 | tf_op jit(solution)/shard_map/all_gather | solution.py:50
  325.2 80.5 %all-gather.20.cloned.1.call-start = ((), (), s32[]{:S(2)}) async-start(), calls=%async_computation.6 | async-start | bytes 1638400 | tf_op jit(solution)/shard_map/all_gather | solution.py:79
  371.5 4.9 %collective-permute-start.2 = (bf16[8,256]{1,0:T(8,128)(2,1)S(1)}, bf16[8,256]{1,0:T(8,128)(2,1)S(1)}, u32[]{:S(2)}, u32[]{:S(2)}) collective-permute-start(bf16[8,256]{1,0:T(8,128)(2,1)S(1)} %get-tuple-element.7), channel_id=1, source_target_pairs={{0,4},{4,8},{8,12},{1,5},{5,9},{9,13},{2,6},{6,10},{10,14},{3,7},{... | collective-permute-start | bytes 12296 | tf_op jit(solution)/shard_map/ppermute | solution.py:17
  374.9 5.5 %collective-permute-start.3 = (bf16[8,256]{1,0:T(8,128)(2,1)S(1)}, bf16[8,256]{1,0:T(8,128)(2,1)S(1)}, u32[]{:S(2)}, u32[]{:S(2)}) collective-permute-start(bf16[8,256]{1,0:T(8,128)(2,1)S(1)} %get-tuple-element.8), channel_id=1, source_target_pairs={{4,0},{8,4},{12,8},{5,1},{9,5},{13,9},{6,2},{10,6},{14,10},{7,3},{... | collective-permute-start | bytes 12296 | tf_op jit(solution)/shard_map/ppermute | solution.py:18
Sparse Core Ops, SparseCore 0:
  8.9 83.4 all-gather.9
  94.0 38.8 all-gather.7
  134.5 80.7 all-gather.11
  216.7 79.1 all-gather.15
  297.3 16.7 all-gather.13
  325.3 41.4 all-gather.17
  388.2 17.3 all-gather.19
where the time goes:
time: 417 us
  waiting for transfers between devices  341 us (82%)
  matrix products  29 us (7%)
  blocking collectives  14.3 us (3%)
  between operations  13.7 us (3%)
  starting transfers between devices  9.78 us (2%)
  other arithmetic  7.59 us (2%)
    all_gather x2, waiting for transfers between devices, local(): piece = lax.all_gather(normed, 'tp', axis=1, tiled=True)  82.1 us
    all_gather x1, waiting for transfers between devices, local(): lax.all_gather(w_out, 'sp', axis=1, tiled=True)  75.1 us
    all_gather x1, waiting for transfers between devices, local(): lax.all_gather(w_pool_in, 'sp', axis=1, tiled=True)  71.2 us
    all_gather x1, waiting for transfers between devices, local(): lax.all_gather(w_pool_gate, 'sp', axis=1, tiled=True)  66.5 us
    all_gather x2, waiting for transfers between devices, local(): lax.all_gather(branch, 'tp', axis=1, tiled=True)  35.8 us
    psum x2, blocking collectives, local(): squares = lax.psum(jnp.sum(resid_f * resid_f, axis=1), 'tp')  14.3 us
    dot_general x2, matrix products, local(): gate_sum = jnp.dot(piece, weight_gate, preferred_element_type=jnp.float32)  10.9 us
    dot_general x2, matrix products, local(): pool_sum = jnp.dot(piece, weight_in, preferred_element_type=jnp.float32)  9.35 us
  transfers between devices with their start and end apart: 11, of which 9 were waited for; matrix products, arithmetic and copies ran while one was open for 4% of the time, Pallas kernels for 0%

commit v1 on v0

--- a/solution.py
+++ b/solution.py
@@ -5,6 +5,16 @@
 
 GROUP = 64
 norm_eps = 1e-06
+
+
+def pass_along(shard, mesh_axis, dim):
+    size = lax.axis_size(mesh_axis)
+    held, blocks = (shard, [shard])
+    for _ in range(size - 1):
+        held = lax.ppermute(held, mesh_axis, [(i, (i + 1) % size) for i in range(size)])
+        blocks.insert(0, held)
+    row_of_blocks = jnp.concatenate(blocks, axis=dim)
+    return jnp.roll(row_of_blocks, (lax.axis_index(mesh_axis) + 1) * shard.shape[dim], axis=dim)
 
 
 def with_halo(array, sides, width):
@@ -47,7 +57,7 @@
         scaling = lax.rsqrt(squares / full_width + norm_eps)
         own_gain = lax.dynamic_slice_in_dim(norm_gain[layer], col_rank * col_count, col_count)
         normed = (resid_f * scaling[:, None] * own_gain[None, :]).astype(jnp.bfloat16)
-        piece = lax.all_gather(normed, "tp", axis=1, tiled=True)
+        piece = pass_along(normed, "tp", 1)
         pool_sum = jnp.dot(piece, weight_in, preferred_element_type=jnp.float32)
         gate_sum = jnp.dot(piece, weight_gate, preferred_element_type=jnp.float32)
         pool_in = pool_sum.astype(jnp.bfloat16)

time: 417 us -> 392 us (0.940)
  waiting for transfers between devices: 341 us -> 301 us
  other arithmetic: 7.59 us -> 25.1 us
    ppermute x0 -> x6, waiting for transfers between devices: none -> 102 us  [pass_along(): lax.ppermute(held, mesh_axis, [(i, (i + 1) % size) for i in range(size)])]
    all_gather x2 -> x0, waiting for transfers between devices: 82.1 us -> none  [local(): piece = lax.all_gather(normed, 'tp', axis=1, tiled=True)]
    all_gather x1, waiting for transfers between devices: 71.2 us -> 10.4 us  [local(): lax.all_gather(w_pool_in, 'sp', axis=1, tiled=True)]
    concatenate x0 -> x2, other arithmetic: none -> 19.7 us  [pass_along(): jnp.roll(row_of_blocks, (lax.axis_index(mesh_axis) + 1) * shard.shape[dim...]
  transfers between devices with their start and end apart: 11 -> 15, of which waited for: 9 -> 13; matrix products, arithmetic and copies ran while one was open for 4% -> 7% of each run, Pallas kernels for 0% -> 0%
where the time goes in v1:
time: 392 us; the launch traced here: 391 us
  waiting for transfers between devices  301 us (77%)
  matrix products  26.7 us (7%)
  other arithmetic  25.1 us (6%)
  blocking collectives  14.3 us (4%)
  between operations  13.4 us (3%)
  starting transfers between devices  7.7 us (2%)
    ppermute x6, waiting for transfers between devices, pass_along(): lax.ppermute(held, mesh_axis, [(i, (i + 1) % size) for i in range(size)])  102 us
    all_gather x1, waiting for transfers between devices, local(): lax.all_gather(w_out, 'sp', axis=1, tiled=True)  75.3 us
    all_gather x1, waiting for transfers between devices, local(): lax.all_gather(w_pool_gate, 'sp', axis=1, tiled=True)  66.2 us
    all_gather x2, waiting for transfers between devices, local(): lax.all_gather(branch, 'tp', axis=1, tiled=True)  36.7 us
    concatenate x2, other arithmetic, pass_along(): jnp.roll(row_of_blocks, (lax.axis_index(mesh_axis) + 1) * shard.shape[dim...  19.7 us
    psum x2, blocking collectives, local(): squares = lax.psum(jnp.sum(resid_f * resid_f, axis=1), 'tp')  14.3 us
    dot_general x2, matrix products, local(): gate_sum = jnp.dot(piece, weight_gate, preferred_element_type=jnp.float32)  10.9 us
    all_gather x1, waiting for transfers between devices, local(): lax.all_gather(w_pool_in, 'sp', axis=1, tiled=True)  10.4 us
  transfers between devices with their start and end apart: 15, of which 13 were waited for; matrix products, arithmetic and copies ran while one was open for 7% of the time, Pallas kernels for 0%

profile of v1, /device:TPU:0, one launch (start us, length us, event | category | flops | bytes accessed | tf_op | source)
XLA Modules:
  0.0 391.1 jit_solution(17403973731508083218)
XLA Ops:
  8.1 1.6 fusion.14
  9.7 8.4 %psum.14 = f32[640]{0:T(1024)S(1)} all-reduce(f32[640]{0:T(1024)S(1)} %fusion.14), channel_id=1, replica_groups=mesh['grp'=2,'sp'=4,'tp'=4] {'tp'}, use_global_device_ids=true, to_apply=%region_1.2 | all-reduce | flops 640 | bytes 5120 | tf_op jit(solution)/shard_map/psum | solution.py:56
  18.1 0.9 fusion.55
  19.4 17.1 %collective-permute-done = bf16[640,1024]{1,0:T(8,128)(2,1)} collective-permute-done((bf16[640,1024]{1,0:T(8,128)(2,1)S(1)}, bf16[640,1024]{1,0:T(8,128)(2,1)}, u32[]{:S(2)}, u32[]{:S(2)}) %collective-permute-start) | collective-permute-done | bytes 1310752 | tf_op jit(solution)/shard_map/ppermute | solution.py:14
  36.6 17.3 %collective-permute-done.1 = bf16[640,1024]{1,0:T(8,128)(2,1)} collective-permute-done((bf16[640,1024]{1,0:T(8,128)(2,1)}, bf16[640,1024]{1,0:T(8,128)(2,1)}, u32[]{:S(2)}, u32[]{:S(2)}) %collective-permute-start.1) | collective-permute-done | bytes 1310752 | tf_op jit(solution)/shard_map/ppermute | solution.py:14
  54.7 16.5 %collective-permute-done.2 = bf16[640,1024]{1,0:T(8,128)(2,1)} collective-permute-done((bf16[640,1024]{1,0:T(8,128)(2,1)}, bf16[640,1024]{1,0:T(8,128)(2,1)}, u32[]{:S(2)}, u32[]{:S(2)}) %collective-permute-start.2) | collective-permute-done | bytes 1310752 | tf_op jit(solution)/shard_map/ppermute | solution.py:14
  71.2 10.7 %fusion.10 = bf16[640,4096]{1,0:T(8,128)(2,1)} fusion(s32[]{:T(128)S(6)} %select_n.95, bf16[640,1024]{1,0:T(8,128)(2,1)} %collective-permute-done.2, bf16[640,1024]{1,0:T(8,128)(2,1)} %collective-permute-done.1, bf16[640,1024]{1,0:T(8,128)(2,1)} %collective-permute-done, bf16[640,1024]{1,0:T(8,128)(2,1)S(1)} %fusion.16), kind=kLoop, calls=%fused_computation.26 | loop fusion | flops 41943040 | bytes 10485764 | tf_op jit(solution)/shard_map/jit(_roll_dynamic)/concatenate | solution.py:17
  82.0 10.4 %all-gather.6.cloned.1.call-done = bf16[2,4096,256]{2,1,0:T(8,128)(2,1)} async-done(((bf16[2,1024,256]{2,1,0:T(8,128)(2,1)}), bf16[2,4096,256]{2,1,0:T(8,128)(2,1)}) %all-gather.6.cloned.1.call-update) | async-done | bytes 4194320 | tf_op jit(solution)/shard_map/all_gather | solution.py:46
  92.4 4.7 %fusion.28 = bf16[640,256]{1,0:T(8,128)(2,1)S(1)} fusion(bf16[640,4096]{1,0:T(8,128)(2,1)} %fusion.10, bf16[2,4096,256]{2,1,0:T(8,128)(2,1)} %all-gather.6.cloned.1.call-done), kind=kOutput, calls=%fused_computation.56 | convolution fusion | flops 1342341120 | bytes 7667712 | tf_op jit(solution)/shard_map/dot_general | solution.py:61
  97.1 1.3 collective-permute-start.3
  98.4 1.3 collective-permute-start.4
  99.7 4.3 %collective-permute-done.4 = bf16[8,256]{1,0:T(8,128)(2,1)S(1)} collective-permute-done((bf16[8,256]{1,0:T(8,128)(2,1)S(1)}, bf16[8,256]{1,0:T(8,128)(2,1)S(1)}, u32[]{:S(2)}, u32[]{:S(2)}) %collective-permute-start.4) | collective-permute-done | bytes 4128 | tf_op jit(solution)/shard_map/ppermute | solution.py:28
  104.0 1.5 fusion.40
  105.7 1.1 fusion.44
  107.1 66.2 %all-gather.8.cloned.1.call-done = bf16[2,4096,256]{2,1,0:T(8,128)(2,1)} async-done(((bf16[2,1024,256]{2,1,0:T(8,128)(2,1)}), bf16[2,4096,256]{2,1,0:T(8,128)(2,1)}) %all-gather.8.cloned.1.call-update) | async-done | bytes 4194320 | tf_op jit(solution)/shard_map/all_gather | solution.py:47
  173.3 5.4 %multiply_convert_fusion.1 = bf16[640,256]{1,0:T(8,128)(2,1)} fusion(f32[640,256]{1,0:T(8,128)S(1)} %copy.15, bf16[640,4096]{1,0:T(8,128)(2,1)} %fusion.10, bf16[2,4096,256]{2,1,0:T(8,128)(2,1)} %all-gather.8.cloned.1.call-done), kind=kOutput, calls=%fused_computation.99 | convolution fusion | flops 1343488000 | bytes 8323072 | tf_op jit(solution)/shard_map/dot_general | solution.py:62
  178.8 75.3 %all-gather.12.cloned.1.call-done = bf16[2,1024,1024]{2,1,0:T(8,128)(2,1)} async-done(((bf16[2,256,1024]{2,1,0:T(8,128)(2,1)}), bf16[2,1024,1024]{2,1,0:T(8,128)(2,1)}) %all-gather.12.cloned.1.call-update) | async-done | bytes 4194320 | tf_op jit(solution)/shard_map/all_gather | solution.py:48
  254.1 18.2 %all-gather.10.cloned.1.call-done = bf16[640,1024]{1,0:T(8,128)(2,1)} async-done(((bf16[640,256]{1,0:T(8,128)(2,1)}), bf16[640,1024]{1,0:T(8,128)(2,1)}) %all-gather.10.cloned.1.call-update) | async-done | bytes 1310736 | tf_op jit(solution)/shard_map/all_gather | solution.py:89
  272.3 3.7 fusion.18
  276.0 5.9 %psum.15 = f32[640]{0:T(1024)S(1)} all-reduce(f32[640]{0:T(1024)S(1)} %get-tuple-element.14), channel_id=1, replica_groups=mesh['grp'=2,'sp'=4,'tp'=4] {'tp'}, use_global_device_ids=true, to_apply=%region_3.5 | all-reduce | flops 640 | bytes 5120 | tf_op jit(solution)/shard_map/psum | solution.py:56
  282.3 17.0 %collective-permute-done.5 = bf16[640,1024]{1,0:T(8,128)(2,1)S(1)} collective-permute-done((bf16[640,1024]{1,0:T(8,128)(2,1)S(1)}, bf16[640,1024]{1,0:T(8,128)(2,1)S(1)}, u32[]{:S(2)}, u32[]{:S(2)}) %collective-permute-start.5) | collective-permute-done | bytes 1310752 | tf_op jit(solution)/shard_map/ppermute | solution.py:14
  299.4 17.0 %collective-permute-done.6 = bf16[640,1024]{1,0:T(8,128)(2,1)S(1)} collective-permute-done((bf16[640,1024]{1,0:T(8,128)(2,1)S(1)}, bf16[640,1024]{1,0:T(8,128)(2,1)S(1)}, u32[]{:S(2)}, u32[]{:S(2)}) %collective-permute-start.6) | collective-permute-done | bytes 1310752 | tf_op jit(solution)/shard_map/ppermute | solution.py:14
  316.4 17.0 %collective-permute-done.7 = bf16[640,1024]{1,0:T(8,128)(2,1)S(1)} collective-permute-done((bf16[640,1024]{1,0:T(8,128)(2,1)S(1)}, bf16[640,1024]{1,0:T(8,128)(2,1)S(1)}, u32[]{:S(2)}, u32[]{:S(2)}) %collective-permute-start.7) | collective-permute-done | bytes 1310752 | tf_op jit(solution)/shard_map/ppermute | solution.py:14
  333.4 9.0 %fusion.3 = bf16[640,4096]{1,0:T(8,128)(2,1)S(1)} fusion(s32[]{:T(128)S(6)} %select_n.95, bf16[640,1024]{1,0:T(8,128)(2,1)S(1)} %collective-permute-done.7, bf16[640,1024]{1,0:T(8,128)(2,1)S(1)} %collective-permute-done.6, bf16[640,1024]{1,0:T(8,128)(2,1)S(1)} %collective-permute-done.5, bf16[640,1024]{1,0:T(8,128)(2,1)S(1)} %fusion.20), kind=kLoop, calls=%fused_computation.19 | loop fusion | flops 41943040 | bytes 10485764 | tf_op jit(solution)/shard_map/jit(_roll_dynamic)/concatenate | solution.py:17
  342.4 1.5 fusion.31
  344.8 3.5 collective-permute-start.8
  348.3 1.3 collective-permute-start.9
  349.6 4.2 %collective-permute-done.9 = bf16[8,256]{1,0:T(8,128)(2,1)S(1)} collective-permute-done((bf16[8,256]{1,0:T(8,128)(2,1)S(1)}, bf16[8,256]{1,0:T(8,128)(2,1)S(1)}, u32[]{:S(2)}, u32[]{:S(2)}) %collective-permute-start.9) | collective-permute-done | bytes 4128 | tf_op jit(solution)/shard_map/ppermute | solution.py:28
  353.9 1.5 fusion.41
  356.1 5.4 %multiply_convert_fusion = bf16[640,256]{1,0:T(8,128)(2,1)} fusion(f32[640,256]{1,0:T(8,128)S(1)} %copy.18, bf16[640,4096]{1,0:T(8,128)(2,1)} %copy-done.1, bf16[2,4096,256]{2,1,0:T(8,128)(2,1)} %all-gather.8.cloned.1.call-done), kind=kOutput, calls=%fused_computation.98 | convolution fusion | flops 1343488000 | bytes 8323072 | tf_op jit(solution)/shard_map/dot_general | solution.py:62
  361.5 18.5 %all-gather.14.cloned.1.call-done = bf16[640,1024]{1,0:T(8,128)(2,1)} async-done(((bf16[640,256]{1,0:T(8,128)(2,1)}), bf16[640,1024]{1,0:T(8,128)(2,1)}) %all-gather.14.cloned.1.call-update) | async-done | bytes 1310736 | tf_op jit(solution)/shard_map/all_gather | solution.py:89
  380.0 4.6 %fusion.21 = bf16[640,1024]{1,0:T(8,128)(2,1)} fusion(bf16[640,1024]{1,0:T(8,128)(2,1)S(1)} %get-tuple-element.15, bf16[640,1024]{1,0:T(8,128)(2,1)} %all-gather.14.cloned.1.call-done, bf16[2,1024,1024]{2,1,0:T(8,128)(2,1)} %all-gather.12.cloned.1.call-done), kind=kOutput, calls=%fused_computation.43 | convolution fusion | flops 1344143360 | bytes 6029312 | tf_op jit(solution)/shard_map/dot_general | solution.py:88
  (46 shorter events, 5.4 us)
Async XLA Ops:
  6.5 12.4 %copy-start = (bf16[640,1024]{1,0:T(8,128)(2,1)S(1)}, bf16[640,1024]{1,0:T(8,128)(2,1)}, u32[]{:S(2)}) copy-start(bf16[640,1024]{1,0:T(8,128)(2,1)} %param.8) | copy-start | bytes 3932164
  6.5 47.4 %copy-start.2 = (bf16[2,16,64,64]{3,2,1,0:T(8,128)(2,1)S(1)}, bf16[2,16,64,64]{3,2,1,0:T(8,128)(2,1)}, u32[]{:S(2)}) copy-start(bf16[2,16,64,64]{3,2,1,0:T(8,128)(2,1)} %param.12) | copy-start | bytes 786436
  6.5 85.9 %all-gather.6.cloned.1.call-start = ((), (), s32[]{:S(2)}) async-start(), calls=%async_computation | async-start | bytes 5242880 | tf_op jit(solution)/shard_map/all_gather | solution.py:46
  7.3 166.0 %all-gather.8.cloned.1.call-start = ((), (), s32[]{:S(2)}) async-start(), calls=%async_computation.1 | async-start | bytes 5242880 | tf_op jit(solution)/shard_map/all_gather | solution.py:47
  8.0 246.1 %all-gather.12.cloned.1.call-start = ((), (), s32[]{:S(2)}) async-start(), calls=%async_computation.3 | async-start | bytes 5242880 | tf_op jit(solution)/shard_map/all_gather | solution.py:48
  19.4 17.2 %collective-permute-start = (bf16[640,1024]{1,0:T(8,128)(2,1)S(1)}, bf16[640,1024]{1,0:T(8,128)(2,1)}, u32[]{:S(2)}, u32[]{:S(2)}) collective-permute-start(bf16[640,1024]{1,0:T(8,128)(2,1)S(1)} %fusion.16), channel_id=1, source_target_pairs={{0,1},{1,2},{2,3},{3,0},{4,5},{5,6},{6,7},{7,4},{8,9},{9,10},{10,1... | collective-permute-start | bytes 3932168 | tf_op jit(solution)/shard_map/ppermute | solution.py:14
  36.5 17.3 %collective-permute-start.1 = (bf16[640,1024]{1,0:T(8,128)(2,1)}, bf16[640,1024]{1,0:T(8,128)(2,1)}, u32[]{:S(2)}, u32[]{:S(2)}) collective-permute-start(bf16[640,1024]{1,0:T(8,128)(2,1)} %collective-permute-done), channel_id=1, source_target_pairs={{0,1},{1,2},{2,3},{3,0},{4,5},{5,6},{6,7},{7,4},{8,9},{9,10},{10,1... | collective-permute-start | bytes 3932168 | tf_op jit(solution)/shard_map/ppermute | solution.py:14
  36.6 235.7 %all-gather.10.cloned.1.call-start = ((), (), s32[]{:S(2)}) async-start(), calls=%async_computation.2 | async-start | bytes 1638400 | tf_op jit(solution)/shard_map/all_gather | solution.py:89
  53.9 17.3 %collective-permute-start.2 = (bf16[640,1024]{1,0:T(8,128)(2,1)}, bf16[640,1024]{1,0:T(8,128)(2,1)}, u32[]{:S(2)}, u32[]{:S(2)}) collective-permute-start(bf16[640,1024]{1,0:T(8,128)(2,1)} %collective-permute-done.1), channel_id=1, source_target_pairs={{0,1},{1,2},{2,3},{3,0},{4,5},{5,6},{6,7},{7,4},{8,9},{9,10},{10,1... | collective-permute-start | bytes 3932168 | tf_op jit(solution)/shard_map/ppermute | solution.py:14
  97.1 2.6 collective-permute-start.3
  98.4 5.6 %collective-permute-start.4 = (bf16[8,256]{1,0:T(8,128)(2,1)S(1)}, bf16[8,256]{1,0:T(8,128)(2,1)S(1)}, u32[]{:S(2)}, u32[]{:S(2)}) collective-permute-start(bf16[8,256]{1,0:T(8,128)(2,1)S(1)} %get-tuple-element.11), channel_id=1, source_target_pairs={{4,0},{8,4},{12,8},{5,1},{9,5},{13,9},{6,2},{10,6},{14,10},{7,3},{... | collective-permute-start | bytes 12296 | tf_op jit(solution)/shard_map/ppermute | solution.py:28
  178.7 201.3 %all-gather.14.cloned.1.call-start = ((), (), s32[]{:S(2)}) async-start(), calls=%async_computation.4 | async-start | bytes 1638400 | tf_op jit(solution)/shard_map/all_gather | solution.py:89
  282.3 60.1 %copy-start.3 = (bf16[2,4096,256]{2,1,0:T(8,128)(2,1)S(1)}, bf16[2,4096,256]{2,1,0:T(8,128)(2,1)}, u32[]{:S(2)}) copy-start(bf16[2,4096,256]{2,1,0:T(8,128)(2,1)} %all-gather.6.cloned.1.call-done) | copy-start | bytes 12582916
  282.3 17.1 %collective-permute-start.5 = (bf16[640,1024]{1,0:T(8,128)(2,1)S(1)}, bf16[640,1024]{1,0:T(8,128)(2,1)S(1)}, u32[]{:S(2)}, u32[]{:S(2)}) collective-permute-start(bf16[640,1024]{1,0:T(8,128)(2,1)S(1)} %fusion.20), channel_id=1, source_target_pairs={{0,1},{1,2},{2,3},{3,0},{4,5},{5,6},{6,7},{7,4},{8,9},{9,10},{10,1... | collective-permute-start | bytes 3932168 | tf_op jit(solution)/shard_map/ppermute | solution.py:14
  299.4 17.0 %collective-permute-start.6 = (bf16[640,1024]{1,0:T(8,128)(2,1)S(1)}, bf16[640,1024]{1,0:T(8,128)(2,1)S(1)}, u32[]{:S(2)}, u32[]{:S(2)}) collective-permute-start(bf16[640,1024]{1,0:T(8,128)(2,1)S(1)} %collective-permute-done.5), channel_id=1, source_target_pairs={{0,1},{1,2},{2,3},{3,0},{4,5},{5,6},{6,7},{7,4},{8,9},{9,10},{10,1... | collective-permute-start | bytes 3932168 | tf_op jit(solution)/shard_map/ppermute | solution.py:14
  316.4 17.0 %collective-permute-start.7 = (bf16[640,1024]{1,0:T(8,128)(2,1)S(1)}, bf16[640,1024]{1,0:T(8,128)(2,1)S(1)}, u32[]{:S(2)}, u32[]{:S(2)}) collective-permute-start(bf16[640,1024]{1,0:T(8,128)(2,1)S(1)} %collective-permute-done.6), channel_id=1, source_target_pairs={{0,1},{1,2},{2,3},{3,0},{4,5},{5,6},{6,7},{7,4},{8,9},{9,10},{10,1... | collective-permute-start | bytes 3932168 | tf_op jit(solution)/shard_map/ppermute | solution.py:14
  342.4 2.3 copy-start.1
  344.8 4.9 %collective-permute-start.8 = (bf16[8,256]{1,0:T(8,128)(2,1)S(1)}, bf16[8,256]{1,0:T(8,128)(2,1)S(1)}, u32[]{:S(2)}, u32[]{:S(2)}) collective-permute-start(bf16[8,256]{1,0:T(8,128)(2,1)S(1)} %get-tuple-element.8), channel_id=1, source_target_pairs={{0,4},{4,8},{8,12},{1,5},{5,9},{9,13},{2,6},{6,10},{10,14},{3,7},{... | collective-permute-start | bytes 12296 | tf_op jit(solution)/shard_map/ppermute | solution.py:27
  348.3 5.5 %collective-permute-start.9 = (bf16[8,256]{1,0:T(8,128)(2,1)S(1)}, bf16[8,256]{1,0:T(8,128)(2,1)S(1)}, u32[]{:S(2)}, u32[]{:S(2)}) collective-permute-start(bf16[8,256]{1,0:T(8,128)(2,1)S(1)} %get-tuple-element.9), channel_id=1, source_target_pairs={{4,0},{8,4},{12,8},{5,1},{9,5},{13,9},{6,2},{10,6},{14,10},{7,3},{... | collective-permute-start | bytes 12296 | tf_op jit(solution)/shard_map/ppermute | solution.py:28
Sparse Core Ops, SparseCore 0:
  8.9 83.4 all-gather.5
  94.0 79.2 all-gather.7
  174.9 79.1 all-gather.11
  255.5 16.7 all-gather.9
  361.7 18.2 all-gather.13
